TPU v7x, 32 devices: a whole 2x2x4 slice. The times are simulated.
32 devices in a mesh: sp: 16 (over z, y, x), tp: 2 (over core).
Axes of the slice: x: 2, y: 2, z: 4, core: 2. Of those that a mesh axis runs over, the one named last changes fastest.
Arguments:
- tokens_in: bfloat16 [4096, 2048], P('sp', 'tp'), may hold values from -720 to 720
- norm_gain: float32 [2048], replicated, may hold values from 0.1 to 1.9
- recept_weight: bfloat16 [2048, 2048], P('sp', 'tp'), may hold values from -0.125 to 0.125
- key_weight: bfloat16 [2048, 2048], P('sp', 'tp'), may hold values from -0.125 to 0.125
- value_weight: bfloat16 [2048, 2048], P('sp', 'tp'), may hold values from -0.125 to 0.125
- decay_weight: bfloat16 [2048, 2048], P('sp', 'tp'), may hold values from -0.0625 to 0.0625
- outer_weight: bfloat16 [2048, 2048], P('sp', 'tp'), may hold values from -0.125 to 0.125
- inner_weight: bfloat16 [2048, 2048], P('sp', 'tp'), may hold values from -0.125 to 0.125
- conv_weight: bfloat16 [2048, 2048], P('sp', 'tp'), may hold values from -0.125 to 0.125
- conv_taps: bfloat16 [3, 2048], P(None, 'tp'), may hold values from -3.5 to 3.5
- decay_base: float32 [2048], P('tp'), may hold values from -12 to -2
- decay_shift: float32 [4096, 2048], P('sp', 'tp'), may hold values from -1 to 12
- rate_logit: float32 [2048], P('tp'), may hold values from -12 to 2
- head_gain: float32 [2048], P('tp'), may hold values from 0.1 to 1.9
- readout_projector: bfloat16 [4096, 2048], P('sp', 'tp'), may hold values from -0.09375 to 0.09375
Outputs:
- mixed: bfloat16 [4096, 2048], P('sp', 'tp')
All inputs are finite; a program needn't handle non-finite values.
Results may differ from a plain program's by a relative error of at most 0.015.
Values may be sent and summed in bfloat16 or wider, within the bound.
A program may use at most 128 MiB of HBM per device.

v0:
```python
import jax
import jax.numpy as jnp
from jax import lax
from jax.sharding import PartitionSpec as P

HEAD_SIZE = 64


norm_eps = 1e-05
group_eps = 0.00064
unit_eps = 1e-06
highest = lax.Precision.HIGHEST


def prefix_2(shard, axis, join, neutral):
    place = lax.axis_index(axis)
    gathered = jax.tree.map(
        lambda a, kind: lax.all_gather(a.astype(kind), axis),
        shard,
        jax.tree.map(lambda a: jnp.bfloat16 if a.dtype == jnp.float32 else a.dtype, shard),
    )
    state = jax.tree.map(lambda a, e: jnp.zeros_like(a) + jnp.asarray(e, a.dtype), shard, neutral)

    def one(hop, state):
        return join(
            state,
            jax.tree.map(
                lambda a, own: lax.dynamic_index_in_dim(a, hop, 0, False).astype(own.dtype),
                gathered,
                shard,
            ),
        )

    return lax.fori_loop(0, place, one, state)


def shifted(value, axis, steps):
    count = lax.axis_size(axis)
    first, last = (max(0, -steps), min(count, count - steps))
    return lax.ppermute(value, axis, [(source, source + steps) for source in range(first, last)])


def compose(earlier, later):
    return (
        jnp.einsum("hij,hjk->hik", earlier[0], later[0], precision=highest),
        jnp.einsum("hij,hjk->hik", earlier[1], later[0], precision=highest) + later[1],
    )


def state_mixer(recept, keys, values, decay_proj, decay_base, decay_shift, rate_logit, head_gain):
    rows, cols = recept.shape
    heads = cols // HEAD_SIZE
    span = min(64, rows // 2)
    blocks = rows // span
    pre = decay_base + decay_proj.astype(jnp.float32) + decay_shift
    log_decay = -jnp.exp(-jax.nn.softplus(-pre) - 0.5)
    rate = jax.nn.sigmoid(rate_logit).reshape(heads, HEAD_SIZE)

    def blocked(array):
        return array.astype(jnp.float32).reshape(blocks, span, heads, HEAD_SIZE)

    query_rows = blocked(recept)
    key_rows = blocked(keys)
    value_rows = blocked(values)
    decay_rows = blocked(log_decay)
    unit = key_rows * lax.rsqrt(jnp.sum(key_rows * key_rows, axis=-1, keepdims=True) + unit_eps)
    beta_rows = unit * rate
    running = jnp.cumsum(decay_rows, axis=1)
    before = running - decay_rows
    closing_position = running[:, -1:]
    query_dec = query_rows * jnp.exp(running)
    alpha_dec = -unit * jnp.exp(before)
    key_inv = key_rows * jnp.exp(-running)
    inverse_beta_matrix = beta_rows * jnp.exp(-running)
    key_end = key_rows * jnp.exp(closing_position - running)
    beta_end = beta_rows * jnp.exp(closing_position - running)
    order = jnp.arange(span)
    exclusive_triangle = order[:, None] > order[None, :]
    inclusive = order[:, None] >= order[None, :]

    def pairs(left, right, mask):
        inner = jnp.einsum("bthn,bshn->bhts", left, right, precision=highest)
        return jnp.where(mask, inner, 0.0)

    alpha_beta = pairs(alpha_dec, inverse_beta_matrix, exclusive_triangle)
    alpha_key = pairs(alpha_dec, key_inv, exclusive_triangle)
    query_beta = pairs(query_dec, inverse_beta_matrix, inclusive)
    query_key = pairs(query_dec, key_inv, inclusive)
    value_heads = jnp.swapaxes(value_rows, 1, 2)
    right_side = jnp.concatenate(
        [
            jnp.swapaxes(alpha_dec, 1, 2),
            jnp.einsum("bhts,bhsn->bhtn", alpha_key, value_heads, precision=highest),
        ],
        axis=-1,
    )
    eye_span = jnp.eye(span, dtype=jnp.float32)
    solved = jax.scipy.linalg.solve_triangular(eye_span - alpha_beta, right_side, lower=True)
    mixing = solved[..., :HEAD_SIZE]
    base_rows = solved[..., HEAD_SIZE:]
    eye_head = jnp.eye(HEAD_SIZE, dtype=jnp.float32)
    transfer = jnp.exp(closing_position[:, 0])[..., None] * eye_head + jnp.einsum(
        "bhtk,bthj->bhkj", mixing, beta_end, precision=highest
    )
    added = jnp.einsum("bhtv,bthk->bhvk", base_rows, beta_end, precision=highest) + jnp.einsum(
        "bthv,bthk->bhvk", value_rows, key_end, precision=highest
    )
    query_all = jnp.swapaxes(query_dec, 1, 2) + jnp.einsum(
        "bhts,bhsk->bhtk", query_beta, mixing, precision=highest
    )
    local_read = jnp.einsum(
        "bhts,bhsv->bhtv", query_beta, base_rows, precision=highest
    ) + jnp.einsum("bhts,bhsv->bhtv", query_key, value_heads, precision=highest)
    eye_heads = jnp.broadcast_to(eye_head, (heads, HEAD_SIZE, HEAD_SIZE))
    zero_heads = jnp.zeros((heads, HEAD_SIZE, HEAD_SIZE), jnp.float32)

    def advance(carry, block):
        return (compose(carry, block), carry)

    device_maps, block_maps = lax.scan(advance, (eye_heads, zero_heads), (transfer, added))
    prefix = prefix_2(device_maps, "sp", compose, (eye_heads, zero_heads))
    entering = prefix[1]
    starts = (
        jnp.einsum("hvk,bhkj->bhvj", entering, block_maps[0], precision=highest) + block_maps[1]
    )
    reads = jnp.einsum("bhtk,bhvk->bhtv", query_all, starts, precision=highest) + local_read
    center = jnp.mean(reads, axis=-1, keepdims=True)
    variance = jnp.mean(jnp.square(reads - center), axis=-1, keepdims=True)
    normalized_rows = jnp.swapaxes(
        (reads - center) * lax.rsqrt(variance + group_eps), 1, 2
    ).reshape(rows, cols)
    return (normalized_rows * head_gain).astype(jnp.bfloat16)


def body(
    tokens_in,
    norm_gain,
    recept_weight,
    key_weight,
    value_weight,
    decay_weight,
    outer_weight,
    inner_weight,
    conv_weight,
    conv_taps,
    decay_base,
    decay_shift,
    rate_logit,
    head_gain,
    readout_projector,
):
    whole = lax.all_gather(tokens_in, "tp", axis=1, tiled=True)
    wide = whole.astype(jnp.float32)
    center = jnp.mean(wide, axis=-1, keepdims=True)
    variance = jnp.mean(jnp.square(wide - center), axis=-1, keepdims=True)
    normalized_rows = ((wide - center) * lax.rsqrt(variance + norm_eps) * norm_gain).astype(
        jnp.bfloat16
    )
    pieces = (
        lax.all_gather(recept_weight, "sp", axis=0, tiled=True),
        lax.all_gather(key_weight, "sp", axis=0, tiled=True),
        lax.all_gather(value_weight, "sp", axis=0, tiled=True),
        lax.all_gather(decay_weight, "sp", axis=0, tiled=True),
        lax.all_gather(outer_weight, "sp", axis=0, tiled=True),
        lax.all_gather(inner_weight, "sp", axis=0, tiled=True),
        lax.all_gather(conv_weight, "sp", axis=0, tiled=True),
    )
    sums = tuple(
        (jnp.dot(normalized_rows, piece, preferred_element_type=jnp.float32) for piece in pieces)
    )
    recept, keys, values, decay_proj, outer, inner, conv_in = tuple(
        (total.astype(jnp.bfloat16) for total in sums)
    )
    gated = (inner.astype(jnp.float32) * conv_in.astype(jnp.float32)).astype(jnp.bfloat16)
    rim = shifted(gated[-2:], "sp", 1)
    padded = jnp.concatenate([rim, gated], axis=0).astype(jnp.float32)
    taps = conv_taps.astype(jnp.float32)
    conv_sum = taps[0] * padded[:-2] + taps[1] * padded[1:-1] + taps[2] * padded[2:]
    conv_branch = (outer.astype(jnp.float32) * conv_sum).astype(jnp.bfloat16)
    state_branch = state_mixer(
        recept, keys, values, decay_proj, decay_base, decay_shift, rate_logit, head_gain
    )
    output_rows = lax.all_gather(readout_projector, "sp", axis=0, tiled=True)
    half = output_rows.shape[0] // 2
    pieces = (
        lax.all_gather(conv_branch, "tp", axis=1, tiled=True),
        lax.all_gather(state_branch, "tp", axis=1, tiled=True),
    )
    count = pieces[0].shape[1]
    convolved_token_rows = lax.slice_in_dim(output_rows, 0, count, axis=0)
    state_rows = lax.dynamic_slice_in_dim(output_rows, half, count, 0)
    mixed = jnp.dot(pieces[0], convolved_token_rows, preferred_element_type=jnp.float32) + jnp.dot(
        pieces[1], state_rows, preferred_element_type=jnp.float32
    )
    return mixed.astype(jnp.bfloat16)


def solution(mesh):
    in_specs = (
        P("sp", "tp"),
        P(),
        P("sp", "tp"),
        P("sp", "tp"),
        P("sp", "tp"),
        P("sp", "tp"),
        P("sp", "tp"),
        P("sp", "tp"),
        P("sp", "tp"),
        P(None, "tp"),
        P("tp"),
        P("sp", "tp"),
        P("tp"),
        P("tp"),
        P("sp", "tp"),
    )
    out_specs = P("sp", "tp")
    return jax.shard_map(body, mesh=mesh, in_specs=in_specs, out_specs=out_specs, check_vma=False)
```

profile of v0, /device:TPU:0, one launch (start us, length us, event | category | flops | bytes accessed | tf_op | source)
XLA Modules:
  0.0 1193.5 jit_solution(2346899973656875451)
XLA Ops:
  10.9 9.8 all-gather.16.cloned.1.call-done
  23.9 76.4 %all-gather.32.cloned.1.call-done = bf16[2048,1024]{1,0:T(8,128)(2,1)} async-done(((bf16[128,1024]{1,0:T(8,128)(2,1)}), bf16[2048,1024]{1,0:T(8,128)(2,1)}) %all-gather.32.cloned.1.call-update) | async-done | bytes 4194320 | tf_op jit(solution)/shard_map/all_gather | solution.py:161
  105.6 71.6 %all-gather.30.cloned.1.call-done = bf16[2048,1024]{1,0:T(8,128)(2,1)} async-done(((bf16[128,1024]{1,0:T(8,128)(2,1)}), bf16[2048,1024]{1,0:T(8,128)(2,1)}) %all-gather.30.cloned.1.call-update) | async-done | bytes 4194320 | tf_op jit(solution)/shard_map/all_gather | solution.py:163
  177.2 4.2 fusion.81
  186.3 67.7 %all-gather.34.cloned.1.call-done = bf16[2048,1024]{1,0:T(8,128)(2,1)} async-done(((bf16[128,1024]{1,0:T(8,128)(2,1)}), bf16[2048,1024]{1,0:T(8,128)(2,1)}) %all-gather.34.cloned.1.call-update) | async-done | bytes 4194320 | tf_op jit(solution)/shard_map/all_gather | solution.py:162
  254.1 4.3 convolution_convert_fusion
  260.7 11.2 select_bitcast_fusion
  271.9 316.0 %custom-call.4 = f32[4,16,1,64,64]{3,4,2,1,0:T(8,128)} custom-call(f32[4,16,1,64,64]{4,3,2,1,0:T(8,128)} %select_bitcast_fusion), custom_call_target="InvertDiagBlocksLowerTriangular" | custom-call | tf_op jit(solution)/shard_map/jit(_solve_triangular)/vmap(vmap())/triangular_solve | solution.py:98
  589.8 8.8 fusion.99
  603.2 4.5 fusion.24
  610.2 6.8 multiply_add_fusion
  617.0 7.0 fusion.53
  624.1 40.7 %while.30 = (s32[]{:T(128)}, f32[16,64,64]{1,2,0:T(8,128)S(1)}, f32[16,64,64]{1,2,0:T(8,128)}, f32[4,16,64,64]{2,3,1,0:T(8,128)}, f32[4,16,64,64]{2,3,1,0:T(8,12...) while((s32[]{:T(128)}, f32[16,64,64]{1,2,0:T(8,128)S(1)}, ...), condition=%wide.region_5.6_spmd.clone, body=%wide.region_4.5_spmd.clone.sunk | while | flops 100859904 | bytes 7340188 | solution.py:120
  669.9 4.5 fusion.70
  677.4 8.6 fusion.101
  686.0 3.7 fusion.45
  689.7 5.6 fusion.39
  695.4 7.3 fusion.97
  702.7 37.3 %all-gather.38.cloned.1.call-done = bf16[256,64,64]{2,1,0:T(8,128)(2,1)} async-done(((bf16[16,64,64]{2,1,0:T(8,128)(2,1)}), bf16[256,64,64]{2,1,0:T(8,128)(2,1)}) %all-gather.38.cloned.1.call-update) | async-done | bytes 2097168 | tf_op jit(solution)/shard_map/all_gather | solution.py:18
  740.0 77.0 %all-gather.40.cloned.1.call-done = bf16[256,64,64]{2,1,0:T(8,128)(2,1)} async-done(((bf16[16,64,64]{2,1,0:T(8,128)(2,1)}), bf16[256,64,64]{2,1,0:T(8,128)(2,1)}) %all-gather.40.cloned.1.call-update) | async-done | bytes 2097168 | tf_op jit(solution)/shard_map/all_gather | solution.py:18
  818.1 3.8 fusion.95
  821.9 6.6 fusion.29
  837.4 56.5 %all-gather.20.cloned.1.call-done = bf16[2048,1024]{1,0:T(8,128)(2,1)} async-done(((bf16[128,1024]{1,0:T(8,128)(2,1)}), bf16[2048,1024]{1,0:T(8,128)(2,1)}) %all-gather.20.cloned.1.call-update) | async-done | bytes 4194320 | tf_op jit(solution)/shard_map/all_gather | solution.py:165
  897.5 73.5 %all-gather.22.cloned.1.call-done = bf16[2048,1024]{1,0:T(8,128)(2,1)} async-done(((bf16[128,1024]{1,0:T(8,128)(2,1)}), bf16[2048,1024]{1,0:T(8,128)(2,1)}) %all-gather.22.cloned.1.call-update) | async-done | bytes 4194320 | tf_op jit(solution)/shard_map/all_gather | solution.py:166
  971.0 3.5 fusion.73
  979.3 68.5 %all-gather.18.cloned.1.call-done = bf16[2048,1024]{1,0:T(8,128)(2,1)} async-done(((bf16[128,1024]{1,0:T(8,128)(2,1)}), bf16[2048,1024]{1,0:T(8,128)(2,1)}) %all-gather.18.cloned.1.call-update) | async-done | bytes 4194320 | tf_op jit(solution)/shard_map/all_gather | solution.py:164
  1047.8 4.4 fusion.77
  1052.3 4.7 all-gather.36.cloned.1.call-done
  1057.0 116.1 %all-gather.26.cloned.1.call-done = bf16[4096,1024]{1,0:T(8,128)(2,1)} async-done(((bf16[256,1024]{1,0:T(8,128)(2,1)}), bf16[4096,1024]{1,0:T(8,128)(2,1)}) %all-gather.26.cloned.1.call-update) | async-done | bytes 8388624 | tf_op jit(solution)/shard_map/all_gather | solution.py:183
  1173.1 3.8 fusion.15
  1176.9 5.0 all-gather.24.cloned.1.call-done
  1181.9 4.6 fusion.62
  (153 shorter events, 95.8 us)
Async XLA Ops:
  6.5 93.7 %copy-start.21 = (f32[2048]{0:T(1024)S(1)}, f32[2048]{0:T(1024)}, u32[]{:S(2)}) copy-start(f32[2048]{0:T(1024)} %param.20) | copy-start | bytes 24580
  6.5 14.1 %all-gather.16.cloned.1.call-start = ((), (), s32[]{:S(2)}) async-start(), calls=%async_computation | async-start | bytes 1572864 | tf_op jit(solution)/shard_map/all_gather | solution.py:152
  7.3 93.0 %all-gather.32.cloned.1.call-start = ((), (), s32[]{:S(2)}) async-start(), calls=%async_computation.8 | async-start | bytes 4456448 | tf_op jit(solution)/shard_map/all_gather | solution.py:161
  8.0 169.2 %all-gather.30.cloned.1.call-start = ((), (), s32[]{:S(2)}) async-start(), calls=%async_computation.7 | async-start | bytes 4456448 | tf_op jit(solution)/shard_map/all_gather | solution.py:163
  8.7 245.3 %all-gather.34.cloned.1.call-start = ((), (), s32[]{:S(2)}) async-start(), calls=%async_computation.9 | async-start | bytes 4456448 | tf_op jit(solution)/shard_map/all_gather | solution.py:162
  9.3 660.6 %all-gather.28.cloned.1.call-start = ((), (), s32[]{:S(2)}) async-start(), calls=%async_computation.6 | async-start | bytes 4456448 | tf_op jit(solution)/shard_map/all_gather | solution.py:160
  9.9 730.1 %all-gather.38.cloned.1.call-start = ((), (), s32[]{:S(2)}) async-start(), calls=%async_computation.11 | async-start | bytes 4456448 | tf_op jit(solution)/shard_map/all_gather | solution.py:18
  20.7 79.6 %copy-start.14 = (bf16[256,2048]{1,0:T(8,128)(2,1)S(1)}, bf16[256,2048]{1,0:T(8,128)(2,1)}, u32[]{:S(2)}) copy-start(bf16[256,2048]{1,0:T(8,128)(2,1)} %all-gather.16.cloned.1.call-done) | copy-start | bytes 3145732
  103.7 73.5 %copy-start.20 = (f32[256,1024]{1,0:T(8,128)S(1)}, f32[256,1024]{1,0:T(8,128)}, u32[]{:S(2)}) copy-start(f32[256,1024]{1,0:T(8,128)} %param.30) | copy-start | bytes 3145732
  103.7 73.5 %copy-start.22 = (f32[1024]{0:T(1024)S(1)}, f32[1024]{0:T(1024)}, u32[]{:S(2)}) copy-start(f32[1024]{0:T(1024)} %param.29) | copy-start | bytes 12292
  603.1 4.5 copy-start.9
  607.6 9.4 copy-start.3
  641.4 3.1 copy-start.8
  665.7 4.2 copy-start.15
  665.7 151.3 %all-gather.40.cloned.1.call-start = ((), (), s32[]{:S(2)}) async-start(), calls=%async_computation.12 | async-start | bytes 4456448 | tf_op jit(solution)/shard_map/all_gather | solution.py:18
  667.7 226.2 %all-gather.20.cloned.1.call-start = ((), (), s32[]{:S(2)}) async-start(), calls=%async_computation.2 | async-start | bytes 4456448 | tf_op jit(solution)/shard_map/all_gather | solution.py:165
  668.5 302.5 %all-gather.22.cloned.1.call-start = ((), (), s32[]{:S(2)}) async-start(), calls=%async_computation.3 | async-start | bytes 4456448 | tf_op jit(solution)/shard_map/all_gather | solution.py:166
  669.2 378.6 %all-gather.18.cloned.1.call-start = ((), (), s32[]{:S(2)}) async-start(), calls=%async_computation.1 | async-start | bytes 4456448 | tf_op jit(solution)/shard_map/all_gather | solution.py:164
  669.8 387.2 %all-gather.36.cloned.1.call-start = ((), (), s32[]{:S(2)}) async-start(), calls=%async_computation.10 | async-start | bytes 1572864 | tf_op jit(solution)/shard_map/all_gather | solution.py:187
  677.4 8.6 copy-start.4
  689.7 5.6 copy-start.2
  689.7 5.6 copy-start.6
  818.1 3.8 copy-start.7
  818.1 3.8 copy-start.13
  821.9 6.7 copy-start.10
  821.9 6.7 copy-start.11
  821.9 6.7 copy-start.12
  835.6 58.4 %copy-start.16 = (bf16[256,2048]{1,0:T(8,128)(2,1)S(1)}, bf16[256,2048]{1,0:T(8,128)(2,1)}, u32[]{:S(2)}) copy-start(bf16[256,2048]{1,0:T(8,128)(2,1)} %all-gather.16.cloned.1.call-done) | copy-start | bytes 3145732
  836.5 336.6 %all-gather.26.cloned.1.call-start = ((), (), s32[]{:S(2)}) async-start(), calls=%async_computation.5 | async-start | bytes 8912896 | tf_op jit(solution)/shard_map/all_gather | solution.py:183
  837.1 344.8 %all-gather.24.cloned.1.call-start = ((), (), s32[]{:S(2)}) async-start(), calls=%async_computation.4 | async-start | bytes 1572864 | tf_op jit(solution)/shard_map/all_gather | solution.py:186
  897.5 80.4 %copy-start.18 = (bf16[3,1024]{1,0:T(4,128)(2,1)S(1)}, bf16[3,1024]{1,0:T(4,128)(2,1)}, u32[]{:S(2)}) copy-start(bf16[3,1024]{1,0:T(4,128)(2,1)} %param.28) | copy-start | bytes 18436
  974.5 4.7 collective-permute-start
  (8 other events, 19.6 us)
Sparse Core Ops, SparseCore 0:
  8.9 11.7 all-gather.15
  23.4 76.7 all-gather.31
  103.0 74.1 all-gather.29
  179.8 74.1 all-gather.33
  256.7 75.4 all-gather.27
  665.8 74.0 all-gather.37
  742.7 74.1 all-gather.39
  819.7 74.1 all-gather.19
  896.7 74.1 all-gather.21
  973.6 74.1 all-gather.17
  1049.3 7.6 all-gather.35
  1059.6 113.4 all-gather.25
  1174.7 7.1 all-gather.23
where the time goes:
time: 1200 us; the launch traced here: 1190 us
  waiting for transfers between devices  671 us (56%)
  other arithmetic  331 us (28%)
  matrix products  140 us (12%)
  local copies, waits for them, and re-layouts  32.8 us (3%)
  between operations  14.3 us (1%)
    another operation x1, other arithmetic, state_mixer(): jax.scipy.linalg.solve_triangular(eye_span - alpha_beta, right_side, lowe...  316 us
    all_gather x1, waiting for transfers between devices, body(): output_rows = lax.all_gather(readout_projector, 'sp', axis=0, tiled=True)  116 us
    all_gather x2, waiting for transfers between devices, prefix_2(): lax.all_gather(a.astype(kind), axis)  114 us
    all_gather x1, waiting for transfers between devices, body(): lax.all_gather(key_weight, 'sp', axis=0, tiled=True)  76.4 us
    all_gather x1, waiting for transfers between devices, body(): lax.all_gather(conv_weight, 'sp', axis=0, tiled=True)  73.5 us
    all_gather x1, waiting for transfers between devices, body(): lax.all_gather(decay_weight, 'sp', axis=0, tiled=True)  71.6 us
    all_gather x1, waiting for transfers between devices, body(): lax.all_gather(outer_weight, 'sp', axis=0, tiled=True)  68.5 us
    all_gather x1, waiting for transfers between devices, body(): lax.all_gather(value_weight, 'sp', axis=0, tiled=True)  67.7 us
  transfers between devices with their start and end apart: 14, of which 13 were waited for; matrix products, arithmetic and copies ran while one was open for 42% of the time, Pallas kernels for 0%

commit v1 on v0

--- a/solution.py
+++ b/solution.py
@@ -1,6 +1,8 @@
 import jax
 import jax.numpy as jnp
 from jax import lax
+from jax.experimental import pallas as pl
+from jax.experimental.pallas import tpu as pltpu
 from jax.sharding import PartitionSpec as P
 
 HEAD_SIZE = 64
@@ -132,7 +134,7 @@
     return (normalized_rows * head_gain).astype(jnp.bfloat16)
 
 
-def body(
+def gathered_weights_body(
     tokens_in,
     norm_gain,
     recept_weight,
@@ -195,6 +197,255 @@
     return mixed.astype(jnp.bfloat16)
 
 
+CHUNK = 128
+STEP_CHUNKS = 4
+
+
+def split(a):
+    high = a.astype(jnp.bfloat16)
+    return high, (a - high.astype(jnp.float32)).astype(jnp.bfloat16)
+
+
+def dot3(a, b, dims=((1,), (0,))):
+    def one(x, y):
+        return lax.dot_general(x, y, (dims, ((), ())), preferred_element_type=jnp.float32)
+
+    (ah, al), (bh, bl) = split(a), split(b)
+    return one(ah, bh) + (one(ah, bl) + one(al, bh))
+
+
+def unit_lower_inverse(lower, same_block):
+    size = lower[0].shape[0]
+    eye = jnp.where(same_block(1), 1.0, 0.0)
+    base = [jnp.where(same_block(8), a, 0.0) for a in lower]
+    squares = [dot3(a, a) for a in base]
+    inverse = [eye + a for a in base]
+    inverse = [x + dot3(x, s) for x, s in zip(inverse, squares)]
+    fourth = [dot3(s, s) for s in squares]
+    inverse = [x + dot3(x, s) for x, s in zip(inverse, fourth)]
+    width = 8
+    while width < size:
+        off = jnp.logical_and(same_block(2 * width), jnp.logical_not(same_block(width)))
+        right = [dot3(jnp.where(off, a, 0.0), x) for a, x in zip(lower, inverse)]
+        inverse = [x + dot3(x, r) for x, r in zip(inverse, right)]
+        width *= 2
+    return inverse
+
+
+def mixer_kernel(x_ref, w_ref, shift_ref, vec_ref, out_ref, state_ref, rim_ref):
+    @pl.when(pl.program_id(0) == 0)
+    def _():
+        state_ref[...] = jnp.zeros_like(state_ref)
+        rim_ref[...] = jnp.zeros_like(rim_ref)
+
+    n = HEAD_SIZE
+    rows = out_ref.shape[0]
+    count = rows // CHUNK
+    total = 0.0
+    for i in range(x_ref.shape[1]):
+        tokens = x_ref[:, i].reshape(rows, x_ref.shape[3])
+        total += jnp.dot(tokens, w_ref[i], preferred_element_type=jnp.float32)
+    total = total.astype(jnp.bfloat16).astype(jnp.float32)
+    recept, keys, values, decay_proj, outer, inner, conv_in = (
+        total[:, i * n : (i + 1) * n] for i in range(7)
+    )
+    gated = (inner * conv_in).astype(jnp.bfloat16).astype(jnp.float32)
+    padded = jnp.concatenate([rim_ref[...], gated], axis=0)
+    rim_ref[...] = gated[rows - 8 :]
+    conv_sum = (
+        vec_ref[3:4] * padded[6 : 6 + rows]
+        + vec_ref[4:5] * padded[7 : 7 + rows]
+        + vec_ref[5:6] * gated
+    )
+    conv_branch = outer * conv_sum
+
+    pre = vec_ref[0:1] + decay_proj + shift_ref[...]
+    log_decay = -(0.6065306597126334 / (1.0 + jnp.exp(-pre)))
+    rate = 1.0 / (1.0 + jnp.exp(-vec_ref[1:2]))
+    unit = keys * lax.rsqrt(jnp.sum(keys * keys, axis=-1, keepdims=True) + unit_eps)
+    beta = unit * rate
+    row = lax.broadcasted_iota(jnp.int32, (CHUNK, CHUNK), 0)
+    col = lax.broadcasted_iota(jnp.int32, (CHUNK, CHUNK), 1)
+    inclusive = row >= col
+    strict = row > col
+    triangle = jnp.where(inclusive, 1.0, 0.0)
+
+    def same_block(width):
+        return row // width == col // width
+
+    def cut(a):
+        return [a[g * CHUNK : (g + 1) * CHUNK] for g in range(count)]
+
+    chunks = []
+    for q, k, v, u, b, d in zip(*map(cut, (recept, keys, values, unit, beta, log_decay))):
+        running = jnp.dot(
+            triangle, d, preferred_element_type=jnp.float32, precision=highest
+        )
+        before = running - d
+        middle = running[CHUNK // 2 - 1 : CHUNK // 2]
+        closing = running[CHUNK - 1 :]
+        grow = jnp.exp(middle - running)
+        tail = jnp.exp(closing - running)
+        left = jnp.concatenate(
+            [-u * jnp.exp(before - middle), q * jnp.exp(running - middle)], axis=0
+        )
+        right = jnp.concatenate([b * grow, k * grow], axis=0)
+        ends = jnp.concatenate([b * tail, k * tail], axis=0)
+        chunks.append(
+            (left, right, ends, -u * jnp.exp(before), q * jnp.exp(running), v, jnp.exp(closing))
+        )
+    pairs = [dot3(c[0], c[1], ((1,), (1,))) for c in chunks]
+    alpha_key = [jnp.where(strict, p[:CHUNK, CHUNK:], 0.0) for p in pairs]
+    pulled = [dot3(a, c[5]) for a, c in zip(alpha_key, chunks)]
+    inverse = unit_lower_inverse(
+        [jnp.where(strict, p[:CHUNK, :CHUNK], 0.0) for p in pairs], same_block
+    )
+    solved = [
+        dot3(t, jnp.concatenate([c[3], p], axis=1)) for t, c, p in zip(inverse, chunks, pulled)
+    ]
+    stacked = [
+        jnp.concatenate(
+            [s, jnp.concatenate([jnp.zeros_like(c[5]), c[5]], axis=1)], axis=0
+        )
+        for s, c in zip(solved, chunks)
+    ]
+    both = jnp.concatenate([inclusive, inclusive], axis=1)
+    local = [dot3(jnp.where(both, p[CHUNK:], 0.0), m) for p, m in zip(pairs, stacked)]
+    maps = [dot3(m, c[2], ((0,), (0,))) for m, c in zip(stacked, chunks)]
+    state = state_ref[...]
+    reads = []
+    for c, loc, step in zip(chunks, local, maps):
+        reads.append(dot3(c[4] + loc[:, :n], state, ((1,), (1,))) + loc[:, n:])
+        state = state * c[6] + dot3(state, step[:n]) + step[n:]
+    state_ref[...] = state
+    read = jnp.concatenate(reads, axis=0)
+    read = read - jnp.mean(read, axis=-1, keepdims=True)
+    variance = jnp.mean(read * read, axis=-1, keepdims=True)
+    state_branch = read * lax.rsqrt(variance + group_eps) * vec_ref[2:3]
+    out_ref[...] = jnp.concatenate([conv_branch, state_branch], axis=1).astype(out_ref.dtype)
+
+
+def run_mixer(normed, weights, shift, vectors):
+    blocks, halves, own, depth = normed.shape
+    width = weights.shape[-1]
+    rows = STEP_CHUNKS * CHUNK
+    length = blocks * own
+    return pl.pallas_call(
+        mixer_kernel,
+        grid=(length // rows,),
+        out_shape=jax.ShapeDtypeStruct((length, 2 * HEAD_SIZE), jnp.bfloat16),
+        in_specs=[
+            pl.BlockSpec((rows // own, halves, own, depth), lambda i: (i, 0, 0, 0)),
+            pl.BlockSpec((halves, depth, width), lambda i: (0, 0, 0)),
+            pl.BlockSpec((rows, HEAD_SIZE), lambda i: (i, 0)),
+            pl.BlockSpec((8, HEAD_SIZE), lambda i: (0, 0)),
+        ],
+        out_specs=pl.BlockSpec((rows, 2 * HEAD_SIZE), lambda i: (i, 0)),
+        scratch_shapes=[
+            pltpu.VMEM((HEAD_SIZE, HEAD_SIZE), jnp.float32),
+            pltpu.VMEM((8, HEAD_SIZE), jnp.float32),
+        ],
+        compiler_params=pltpu.CompilerParams(
+            dimension_semantics=("arbitrary",), vmem_limit_bytes=40 * 1024 * 1024
+        ),
+        cost_estimate=pl.CostEstimate(
+            flops=60_000_000_000, bytes_accessed=length * depth * 4, transcendentals=0
+        ),
+    )(normed, weights, shift, vectors)
+
+
+def head_body(
+    tokens_in,
+    norm_gain,
+    recept_weight,
+    key_weight,
+    value_weight,
+    decay_weight,
+    outer_weight,
+    inner_weight,
+    conv_weight,
+    conv_taps,
+    decay_base,
+    decay_shift,
+    rate_logit,
+    head_gain,
+    readout_projector,
+):
+    count = lax.axis_size("sp")
+    halves = lax.axis_size("tp")
+    place = lax.axis_index("sp")
+    side = lax.axis_index("tp")
+    rows, cols = tokens_in.shape
+
+    wide = tokens_in.astype(jnp.float32)
+    part_mean = jnp.mean(wide, axis=-1)
+    part_square = jnp.sum(jnp.square(wide - part_mean[:, None]), axis=-1)
+    parts = lax.all_gather(jnp.stack([part_mean, part_square]), "tp", axis=0)
+    center = jnp.mean(parts[:, 0], axis=0)
+    variance = (
+        jnp.sum(parts[:, 1], axis=0) + cols * jnp.sum(jnp.square(parts[:, 0] - center), axis=0)
+    ) / (cols * halves)
+    gain = lax.dynamic_slice_in_dim(norm_gain, side * cols, cols, 0)
+    normed = (
+        (wide - center[:, None]) * lax.rsqrt(variance + norm_eps)[:, None] * gain
+    ).astype(jnp.bfloat16)
+    normed = lax.all_gather(normed, ("sp", "tp"), axis=0)
+    normed, readout_projector = lax.optimization_barrier((normed, readout_projector))
+    normed = normed.reshape(count, halves, rows, cols)
+
+    weights = jnp.stack(
+        [
+            recept_weight,
+            key_weight,
+            value_weight,
+            decay_weight,
+            outer_weight,
+            inner_weight,
+            conv_weight,
+        ]
+    )
+    kinds, depth = weights.shape[:2]
+    weights = weights.reshape(kinds, depth, count, HEAD_SIZE).transpose(2, 1, 0, 3)
+    weights = weights.reshape(count, depth, kinds * HEAD_SIZE)
+    weights = lax.all_to_all(weights, "sp", 0, 0, tiled=True)
+    weights = weights.reshape(halves, cols, kinds * HEAD_SIZE)
+    shift = decay_shift.reshape(rows, count, HEAD_SIZE).transpose(1, 0, 2)
+    shift = lax.all_to_all(shift, "sp", 0, 0, tiled=True).reshape(count * rows, HEAD_SIZE)
+    vectors = jnp.concatenate(
+        [
+            jnp.stack([decay_base, rate_logit, head_gain]),
+            conv_taps.astype(jnp.float32),
+            jnp.zeros((2, cols), jnp.float32),
+        ]
+    )
+    vectors = lax.dynamic_slice_in_dim(vectors, place * HEAD_SIZE, HEAD_SIZE, 1)
+    branches = run_mixer(normed, weights, shift, vectors)
+    branches = branches.reshape(count, rows, 2 * HEAD_SIZE)
+    branches = lax.all_to_all(branches, "sp", 0, 0, tiled=True)
+    branches = branches.reshape(count, rows, 2, HEAD_SIZE).transpose(1, 2, 0, 3)
+    branches = branches.reshape(rows, 2 * cols)
+    branches = lax.all_gather(branches, "tp", axis=0)
+    output_rows = lax.all_gather(readout_projector, "sp", axis=0, tiled=True)
+    output_rows = output_rows.reshape(2, halves, cols, cols)
+    mixed = 0.0
+    for i in range(halves):
+        for branch in range(2):
+            mixed += jnp.dot(
+                branches[i, :, branch * cols : (branch + 1) * cols],
+                output_rows[branch, i],
+                preferred_element_type=jnp.float32,
+            )
+    return mixed.astype(jnp.bfloat16)
+
+
+def body(*args):
+    rows, cols = args[0].shape
+    count = lax.axis_size("sp")
+    if cols == count * HEAD_SIZE and STEP_CHUNKS * CHUNK % rows == 0:
+        return head_body(*args)
+    return gathered_weights_body(*args)
+
+
 def solution(mesh):
     in_specs = (
         P("sp", "tp"),

time: 1200 us -> 404 us (0.34)
  waiting for transfers between devices: 671 us -> 264 us
  other arithmetic: 331 us -> 4.8 us
  matrix products: 140 us -> 9.94 us
  Pallas kernels: 0 us -> 50.6 us
  blocking collectives: 0 us -> 32.7 us
  local copies, waits for them, and re-layouts: 32.8 us -> 13.3 us
    all_gather x13 -> x3, waiting for transfers between devices: 664 us -> 176 us  [the longest x1 116 us: head_body(): output_rows = lax.all_gather(readout_projector, 'sp', axis=0, tiled=True)]
    another operation x2 -> x0, other arithmetic: 318 us -> none  [the longest x1 316 us: state_mixer(): jax.scipy.linalg.solve_triangular(eye_span - alpha_beta, right_side, lowe...]
    dot_general x30 -> x4, matrix products: 135 us -> 9.94 us  [head_body(): jnp.dot(branches[i, :, branch * cols:(branch + 1) * cols], output_rows[br...]
    all_to_all x0 -> x2, waiting for transfers between devices: none -> 87.4 us  [the longest x1 54.6 us: head_body(): weights = lax.all_to_all(weights, 'sp', 0, 0, tiled=True)]
    pallas_call x0 -> x1, Pallas kernels: none -> 50.6 us  [run_mixer(): pl.pallas_call(mixer_kernel, grid=(length // rows,), out_shape=jax.ShapeD...]
    all_to_all x0 -> x1, blocking collectives: none -> 30.8 us  [head_body(): branches = lax.all_to_all(branches, 'sp', 0, 0, tiled=True)]
    all_to_all x0 -> x2, starting transfers between devices: none -> 14.4 us  [the longest x1 8.34 us: head_body(): lax.all_to_all(shift, 'sp', 0, 0, tiled=True)]
    reshape x6 -> x1, local copies, waits for them, and re-layouts: 13 us -> 0.53 us  [head_body(): branches = branches.reshape(count, rows, 2 * HEAD_SIZE)]
  transfers between devices with their start and end apart: 14 -> 5, of which waited for: 13 -> 5; matrix products, arithmetic and copies ran while one was open for 42% -> 2% of each run, Pallas kernels for 0% -> 0%
where the time goes in v1:
time: 404 us; the launch traced here: 403 us
  waiting for transfers between devices  264 us (65%)
  Pallas kernels  50.6 us (13%)
  blocking collectives  32.7 us (8%)
  starting transfers between devices  14.5 us (4%)
  between operations  13.5 us (3%)
  local copies, waits for them, and re-layouts  13.3 us (3%)
  matrix products  9.94 us (2%)
  other arithmetic  4.8 us (1%)
    all_gather x1, waiting for transfers between devices, head_body(): output_rows = lax.all_gather(readout_projector, 'sp', axis=0, tiled=True)  116 us
    all_to_all x1, waiting for transfers between devices, head_body(): weights = lax.all_to_all(weights, 'sp', 0, 0, tiled=True)  54.6 us
    all_gather x1, waiting for transfers between devices, head_body(): normed = lax.all_gather(normed, ('sp', 'tp'), axis=0)  50.9 us
    pallas_call x1, Pallas kernels, run_mixer(): pl.pallas_call(mixer_kernel, grid=(length // rows,), out_shape=jax.ShapeD...  50.6 us
    all_to_all x1, waiting for transfers between devices, head_body(): lax.all_to_all(shift, 'sp', 0, 0, tiled=True)  32.8 us
    all_to_all x1, blocking collectives, head_body(): branches = lax.all_to_all(branches, 'sp', 0, 0, tiled=True)  30.8 us
    dot_general x4, matrix products, head_body(): jnp.dot(branches[i, :, branch * cols:(branch + 1) * cols], output_rows[br...  9.94 us
    all_to_all x1, starting transfers between devices, head_body(): lax.all_to_all(shift, 'sp', 0, 0, tiled=True)  8.34 us
  transfers between devices with their start and end apart: 5, of which 5 were waited for; matrix products, arithmetic and copies ran while one was open for 2% of the time, Pallas kernels for 0%

profile of v1, /device:TPU:0, one launch (start us, length us, event | category | flops | bytes accessed | tf_op | source)
XLA Modules:
  0.0 402.9 jit_solution(9451306618323526495)
XLA Ops:
  6.5 1.3 convert_reduce_fusion
  7.8 1.3 fusion.9
  9.2 2.0 all-gather.2
  11.2 0.7 dynamic_slice.6
  11.9 2.1 fusion.12
  14.1 1.3 copy.40
  15.5 8.3 %all-to-all-start.1 = ((f32[16,256,64]{1,2,0:T(8,128)}), f32[16,256,64]{1,2,0:T(8,128)S(1)}, u32[]{:S(2)}, u32[]{:S(2)}) async-start(f32[16,256,64]{1,2,0:T(8,128)} %bitcast.16), calls=%async_computation.1 | async-start | bytes 2097152 | tf_op jit(solution)/shard_map/all_to_all | solution.py:413
  23.8 0.2 copy.31
  24.0 0.2 copy.32
  24.2 0.2 copy.33
  24.4 0.2 copy.34
  24.6 0.2 copy.35
  24.7 0.2 copy.36
  25.4 1.4 copy.38
  26.8 32.8 %all-to-all-done.1 = f32[16,256,64]{1,2,0:T(8,128)S(1)} async-done(((f32[16,256,64]{1,2,0:T(8,128)}), f32[16,256,64]{1,2,0:T(8,128)S(1)}, u32[]{:S(2)}, u32[]{:S(2)}) %all-to-all-start.1) | async-done | bytes 1048608 | tf_op jit(solution)/shard_map/all_to_all | solution.py:413
  59.6 6.0 %all-to-all-start = ((bf16[16,128,448]{1,2,0:T(8,128)(2,1)}), bf16[16,128,448]{1,2,0:T(8,128)(2,1)}, u32[]{:S(2)}, u32[]{:S(2)}) async-start(bf16[16,128,448]{1,2,0:T(8,128)(2,1)} %bitcast.13), calls=%async_computation | async-start | bytes 3670016 | tf_op jit(solution)/shard_map/all_to_all | solution.py:410
  65.9 0.6 copy.41
  66.5 54.6 %all-to-all-done = bf16[16,128,448]{1,2,0:T(8,128)(2,1)} async-done(((bf16[16,128,448]{1,2,0:T(8,128)(2,1)}), bf16[16,128,448]{1,2,0:T(8,128)(2,1)}, u32[]{:S(2)}, u32[]{:S(2)}) %all-to-all-start) | async-done | bytes 1835040 | tf_op jit(solution)/shard_map/all_to_all | solution.py:410
  121.0 4.0 copy.39
  125.0 50.9 %all-gather.11.cloned.1.call-done = bf16[8192,1024]{1,0:T(8,128)(2,1)} async-done(((bf16[256,1024]{1,0:T(8,128)(2,1)}), bf16[8192,1024]{1,0:T(8,128)(2,1)}) %all-gather.11.cloned.1.call-update) | async-done | bytes 16777232 | tf_op jit(solution)/shard_map/all_gather | solution.py:392
  176.0 1.6 copy-done
  177.6 50.6 %shard_map.145 = bf16[4096,128]{1,0:T(8,128)(2,1)S(1)} custom-call(bf16[16,2,256,1024]{3,2,1,0:T(8,128)(2,1)} %bitcast.89, bf16[2,1024,448]{2,1,0:T(8,128)(2,1)S(1)} %bitcast.68, f32[4096,64]{1,0:T(8,128)S(1)} %bitcast.67, f32[8,64]{1,0:T(8,128)S(1)} %constant_dynamic-slice_fusion.vec_ref), custom_call_target="tpu_custom_call" | custom-call | flops 60000002048 | bytes 16777216 | tf_op jit(solution)/shard_map/pallas_call | solution.py:333
  228.2 0.5 copy.42
  228.8 30.8 %all_to_all.15 = bf16[16,256,128]{1,2,0:T(8,128)(2,1)S(1)} all-to-all(bf16[16,256,128]{1,2,0:T(8,128)(2,1)S(1)} %copy.42), channel_id=1, replica_groups=mesh['sp'=16,'tp'=2] {'sp'}, dimensions={0} | all-to-all | bytes 2097152 | tf_op jit(solution)/shard_map/all_to_all | solution.py:424
  259.6 1.4 copy.44
  261.1 0.7 all-gather.9.cloned.1.call-update
  261.8 8.3 %all-gather.7.cloned.1.call-done = bf16[2,256,2048]{2,1,0:T(8,128)(2,1)} async-done(((bf16[1,256,2048]{2,1,0:T(8,128)(2,1)}), bf16[2,256,2048]{2,1,0:T(8,128)(2,1)}) %all-gather.7.cloned.1.call-update) | async-done | bytes 2097168 | tf_op jit(solution)/shard_map/all_gather | solution.py:427
  270.1 116.3 %all-gather.9.cloned.1.call-done = bf16[4096,1024]{1,0:T(8,128)(2,1)} async-done(((bf16[256,1024]{1,0:T(8,128)(2,1)}), bf16[4096,1024]{1,0:T(8,128)(2,1)}) %all-gather.9.cloned.1.call-update) | async-done | bytes 8388624 | tf_op jit(solution)/shard_map/all_gather | solution.py:428
  386.4 2.6 fusion.1
  389.0 3.0 fusion.2
  392.0 1.8 fusion
  393.8 2.6 fusion.7
  (50 shorter events, 0.9 us)
Async XLA Ops:
  6.5 7.5 %copy-start.1 = (f32[256,1024]{1,0:T(8,128)S(1)}, f32[256,1024]{1,0:T(8,128)}, u32[]{:S(2)}) copy-start(f32[256,1024]{1,0:T(8,128)} %param.26) | copy-start | bytes 3145732
  6.5 169.4 %all-gather.11.cloned.1.call-start = ((), (), s32[]{:S(2)}) async-start(), calls=%async_computation.5 | async-start | bytes 17301504 | tf_op jit(solution)/shard_map/all_gather | solution.py:392
  14.1 9.7 %copy-start.3 = (bf16[128,1024]{1,0:T(8,128)(2,1)S(1)}, bf16[128,1024]{1,0:T(8,128)(2,1)}, u32[]{:S(2)}) copy-start(bf16[128,1024]{1,0:T(8,128)(2,1)} %param.17) | copy-start | bytes 786436
  14.1 9.9 %copy-start.4 = (bf16[128,1024]{1,0:T(8,128)(2,1)S(1)}, bf16[128,1024]{1,0:T(8,128)(2,1)}, u32[]{:S(2)}) copy-start(bf16[128,1024]{1,0:T(8,128)(2,1)} %param.18) | copy-start | bytes 786436
  15.4 8.7 %copy-start.5 = (bf16[128,1024]{1,0:T(8,128)(2,1)S(1)}, bf16[128,1024]{1,0:T(8,128)(2,1)}, u32[]{:S(2)}) copy-start(bf16[128,1024]{1,0:T(8,128)(2,1)} %param.19) | copy-start | bytes 786436
  15.4 8.9 %copy-start.6 = (bf16[128,1024]{1,0:T(8,128)(2,1)S(1)}, bf16[128,1024]{1,0:T(8,128)(2,1)}, u32[]{:S(2)}) copy-start(bf16[128,1024]{1,0:T(8,128)(2,1)} %param.20) | copy-start | bytes 786436
  15.4 9.1 %copy-start.7 = (bf16[128,1024]{1,0:T(8,128)(2,1)S(1)}, bf16[128,1024]{1,0:T(8,128)(2,1)}, u32[]{:S(2)}) copy-start(bf16[128,1024]{1,0:T(8,128)(2,1)} %param.21) | copy-start | bytes 786436
  15.4 9.3 %copy-start.8 = (bf16[128,1024]{1,0:T(8,128)(2,1)S(1)}, bf16[128,1024]{1,0:T(8,128)(2,1)}, u32[]{:S(2)}) copy-start(bf16[128,1024]{1,0:T(8,128)(2,1)} %param.22) | copy-start | bytes 786436
  15.5 44.1 %all-to-all-start.1 = ((f32[16,256,64]{1,2,0:T(8,128)}), f32[16,256,64]{1,2,0:T(8,128)S(1)}, u32[]{:S(2)}, u32[]{:S(2)}) async-start(f32[16,256,64]{1,2,0:T(8,128)} %bitcast.16), calls=%async_computation.1 | async-start | bytes 2097152 | tf_op jit(solution)/shard_map/all_to_all | solution.py:413
  23.8 1.1 copy-start.9
  26.8 38.9 %copy-start.10 = (bf16[3,1024]{1,0:T(4,128)(2,1)S(1)}, bf16[3,1024]{1,0:T(4,128)(2,1)}, u32[]{:S(2)}) copy-start(bf16[3,1024]{1,0:T(4,128)(2,1)} %param.24) | copy-start | bytes 18436
  26.8 38.9 %copy-start.11 = (f32[1024]{0:T(1024)S(1)}, f32[1024]{0:T(1024)}, u32[]{:S(2)}) copy-start(f32[1024]{0:T(1024)} %param.25) | copy-start | bytes 12292
  26.8 38.9 %copy-start.12 = (f32[1024]{0:T(1024)S(1)}, f32[1024]{0:T(1024)}, u32[]{:S(2)}) copy-start(f32[1024]{0:T(1024)} %param.27) | copy-start | bytes 12292
  26.8 38.9 %copy-start.13 = (f32[1024]{0:T(1024)S(1)}, f32[1024]{0:T(1024)}, u32[]{:S(2)}) copy-start(f32[1024]{0:T(1024)} %param.28) | copy-start | bytes 12292
  59.6 61.4 %all-to-all-start = ((bf16[16,128,448]{1,2,0:T(8,128)(2,1)}), bf16[16,128,448]{1,2,0:T(8,128)(2,1)}, u32[]{:S(2)}, u32[]{:S(2)}) async-start(bf16[16,128,448]{1,2,0:T(8,128)(2,1)} %bitcast.13), calls=%async_computation | async-start | bytes 3670016 | tf_op jit(solution)/shard_map/all_to_all | solution.py:410
  65.6 204.5 %all-gather.7.cloned.1.call-start = ((), (), s32[]{:S(2)}) async-start(), calls=%async_computation.3 | async-start | bytes 3145728 | tf_op jit(solution)/shard_map/all_gather | solution.py:427
  176.0 1.6 copy-start
  261.1 125.4 %all-gather.9.cloned.1.call-start = ((), (), s32[]{:S(2)}) async-start(), calls=%async_computation.4 | async-start | bytes 8912896 | tf_op jit(solution)/shard_map/all_gather | solution.py:428
  386.4 5.6 %copy-start.2 = (bf16[4096,1024]{1,0:T(8,128)(2,1)S(1)}, bf16[4096,1024]{1,0:T(8,128)(2,1)}, u32[]{:S(2)}) copy-start(bf16[4096,1024]{1,0:T(8,128)(2,1)} %all-gather.9.cloned.1.call-done) | copy-start | bytes 25165828
Sparse Core Ops, SparseCore 0:
  14.2 161.7 all-gather.10
  261.2 8.9 all-gather.6
  272.9 113.4 all-gather.8

commit v2 on v1

--- a/solution.py
+++ b/solution.py
@@ -391,6 +391,8 @@
     ).astype(jnp.bfloat16)
     normed = lax.all_gather(normed, ("sp", "tp"), axis=0)
     normed, readout_projector = lax.optimization_barrier((normed, readout_projector))
+    output_rows = lax.all_gather(readout_projector, "sp", axis=0, tiled=True)
+    output_rows = output_rows.reshape(2, halves, cols, cols)
     normed = normed.reshape(count, halves, rows, cols)
 
     weights = jnp.stack(
@@ -424,15 +426,18 @@
     branches = lax.all_to_all(branches, "sp", 0, 0, tiled=True)
     branches = branches.reshape(count, rows, 2, HEAD_SIZE).transpose(1, 2, 0, 3)
     branches = branches.reshape(rows, 2 * cols)
-    branches = lax.all_gather(branches, "tp", axis=0)
-    output_rows = lax.all_gather(readout_projector, "sp", axis=0, tiled=True)
-    output_rows = output_rows.reshape(2, halves, cols, cols)
     mixed = 0.0
-    for i in range(halves):
+    for step in range(halves):
+        if step:
+            turn = [(source, (source + step) % halves) for source in range(halves)]
+            held = lax.ppermute(branches, "tp", turn)
+        else:
+            held = branches
+        owner = lax.rem(side + halves - step, halves)
         for branch in range(2):
             mixed += jnp.dot(
-                branches[i, :, branch * cols : (branch + 1) * cols],
-                output_rows[branch, i],
+                held[:, branch * cols : (branch + 1) * cols],
+                lax.dynamic_index_in_dim(output_rows[branch], owner, 0, False),
                 preferred_element_type=jnp.float32,
             )
     return mixed.astype(jnp.bfloat16)

time: 404 us -> 351 us (0.87)
  waiting for transfers between devices: 264 us -> 227 us
  blocking collectives: 32.7 us -> 1.99 us
  starting transfers between devices: 14.5 us -> 31.6 us
  matrix products: 9.94 us -> 3.78 us
    all_gather x1, waiting for transfers between devices: 116 us -> 0.02 us  [head_body(): output_rows = lax.all_gather(readout_projector, 'sp', axis=0, tiled=True)]
    all_gather x1, waiting for transfers between devices: 50.9 us -> 117 us  [head_body(): normed = lax.all_gather(normed, ('sp', 'tp'), axis=0)]
    all_to_all x1 -> x0, blocking collectives: 30.8 us -> none  [head_body(): branches = lax.all_to_all(branches, 'sp', 0, 0, tiled=True)]
    all_to_all x0 -> x1, waiting for transfers between devices: none -> 22.1 us  [head_body(): branches = lax.all_to_all(branches, 'sp', 0, 0, tiled=True)]
    all_to_all x0 -> x1, starting transfers between devices: none -> 21.5 us  [head_body(): branches = lax.all_to_all(branches, 'sp', 0, 0, tiled=True)]
    all_gather x1 -> x0, waiting for transfers between devices: 8.33 us -> none  [head_body(): branches = lax.all_gather(branches, 'tp', axis=0)]
    dot_general x4, matrix products: 9.94 us -> 3.78 us  [head_body(): jnp.dot(held[:, branch * cols:(branch + 1) * cols], lax.dynamic_index_in_...]
    all_to_all x1, starting transfers between devices: 8.34 us -> 3.98 us  [head_body(): lax.all_to_all(shift, 'sp', 0, 0, tiled=True)]
  transfers between devices with their start and end apart: 5 -> 6, of which waited for: 5 -> 4; matrix products, arithmetic and copies ran while one was open for 2% -> 4% of each run, Pallas kernels for 0% -> 14%
where the time goes in v2:
time: 351 us
  waiting for transfers between devices  227 us (65%)
  Pallas kernels  50.6 us (14%)
  starting transfers between devices  31.6 us (9%)
  local copies, waits for them, and re-layouts  16.6 us (5%)
  between operations  13.7 us (4%)
  other arithmetic  4.81 us (1%)
  matrix products  3.78 us (1%)
    all_gather x1, waiting for transfers between devices, head_body(): normed = lax.all_gather(normed, ('sp', 'tp'), axis=0)  117 us
    all_to_all x1, waiting for transfers between devices, head_body(): weights = lax.all_to_all(weights, 'sp', 0, 0, tiled=True)  55.4 us
    pallas_call x1, Pallas kernels, run_mixer(): pl.pallas_call(mixer_kernel, grid=(length // rows,), out_shape=jax.ShapeD...  50.6 us
    all_to_all x1, waiting for transfers between devices, head_body(): lax.all_to_all(shift, 'sp', 0, 0, tiled=True)  32.8 us
    all_to_all x1, waiting for transfers between devices, head_body(): branches = lax.all_to_all(branches, 'sp', 0, 0, tiled=True)  22.1 us
    all_to_all x1, starting transfers between devices, head_body(): branches = lax.all_to_all(branches, 'sp', 0, 0, tiled=True)  21.5 us
  transfers between devices with their start and end apart: 6, of which 4 were waited for; matrix products, arithmetic and copies ran while one was open for 4% of the time, Pallas kernels for 14%

profile of v2, /device:TPU:0, one launch (start us, length us, event | category | flops | bytes accessed | tf_op | source)
XLA Modules:
  0.0 350.5 jit_solution(17684506156401659595)
XLA Ops:
  6.5 1.3 convert_reduce_fusion
  7.8 1.3 fusion.25
  9.2 2.0 all-gather.2
  11.2 0.7 dynamic_slice.19
  11.9 2.1 fusion.28
  14.1 117.0 %all-gather.8.cloned.1.call-done = bf16[8192,1024]{1,0:T(8,128)(2,1)} async-done(((bf16[256,1024]{1,0:T(8,128)(2,1)}), bf16[8192,1024]{1,0:T(8,128)(2,1)}) %all-gather.8.cloned.1.call-update) | async-done | bytes 16777232 | tf_op jit(solution)/shard_map/all_gather | solution.py:392
  131.2 1.3 copy.40
  132.5 4.0 %all-to-all-start.1 = ((f32[16,256,64]{1,2,0:T(8,128)}), f32[16,256,64]{1,2,0:T(8,128)S(1)}, u32[]{:S(2)}, u32[]{:S(2)}) async-start(f32[16,256,64]{1,2,0:T(8,128)} %bitcast.16), calls=%async_computation.1 | async-start | bytes 2097152 | tf_op jit(solution)/shard_map/all_to_all | solution.py:415
  136.5 0.2 copy.31
  136.7 0.2 copy.32
  136.9 0.2 copy.33
  137.1 0.2 copy.34
  137.3 0.2 copy.35
  137.5 0.2 copy.36
  137.6 0.2 copy.37
  138.1 1.4 copy.38
  139.5 32.8 %all-to-all-done.1 = f32[16,256,64]{1,2,0:T(8,128)S(1)} async-done(((f32[16,256,64]{1,2,0:T(8,128)}), f32[16,256,64]{1,2,0:T(8,128)S(1)}, u32[]{:S(2)}, u32[]{:S(2)}) %all-to-all-start.1) | async-done | bytes 1048608 | tf_op jit(solution)/shard_map/all_to_all | solution.py:415
  172.4 6.1 %all-to-all-start = ((bf16[16,128,448]{1,2,0:T(8,128)(2,1)}), bf16[16,128,448]{1,2,0:T(8,128)(2,1)}, u32[]{:S(2)}, u32[]{:S(2)}) async-start(bf16[16,128,448]{1,2,0:T(8,128)(2,1)} %bitcast.13), calls=%async_computation | async-start | bytes 3670016 | tf_op jit(solution)/shard_map/all_to_all | solution.py:412
  178.6 0.6 copy.41
  179.2 55.4 %all-to-all-done = bf16[16,128,448]{1,2,0:T(8,128)(2,1)} async-done(((bf16[16,128,448]{1,2,0:T(8,128)(2,1)}), bf16[16,128,448]{1,2,0:T(8,128)(2,1)}, u32[]{:S(2)}, u32[]{:S(2)}) %all-to-all-start) | async-done | bytes 1835040 | tf_op jit(solution)/shard_map/all_to_all | solution.py:412
  234.6 4.0 %copy.39 = bf16[16,128,448]{2,1,0:T(8,128)(2,1)} copy(bf16[16,128,448]{1,2,0:T(8,128)(2,1)} %all-to-all-done) | data formatting | bytes 3670016 | tf_op jit(solution)/shard_map/all_to_all | solution.py:412
  238.6 1.6 copy-done
  240.2 50.6 %shard_map.145 = bf16[4096,128]{1,0:T(8,128)(2,1)S(1)} custom-call(bf16[16,2,256,1024]{3,2,1,0:T(8,128)(2,1)} %bitcast.80, bf16[2,1024,448]{2,1,0:T(8,128)(2,1)S(1)} %bitcast.57, f32[4096,64]{1,0:T(8,128)S(1)} %bitcast.56, f32[8,64]{1,0:T(8,128)S(1)} %constant_dynamic-slice_fusion.vec_ref), custom_call_target="tpu_custom_call" | custom-call | flops 60000002048 | bytes 16777216 | tf_op jit(solution)/shard_map/pallas_call | solution.py:333
  290.9 1.3 copy.42
  292.2 21.5 %all-to-all-start.2 = ((bf16[16,256,128]{1,2,0:T(8,128)(2,1)}), bf16[16,256,128]{1,2,0:T(8,128)(2,1)S(1)}, u32[]{:S(2)}, u32[]{:S(2)}) async-start(bf16[16,256,128]{1,2,0:T(8,128)(2,1)} %copy.42), calls=%async_computation.2 | async-start | bytes 2097152 | tf_op jit(solution)/shard_map/all_to_all | solution.py:426
  313.7 22.1 %all-to-all-done.2 = bf16[16,256,128]{1,2,0:T(8,128)(2,1)S(1)} async-done(((bf16[16,256,128]{1,2,0:T(8,128)(2,1)}), bf16[16,256,128]{1,2,0:T(8,128)(2,1)S(1)}, u32[]{:S(2)}, u32[]{:S(2)}) %all-to-all-start.2) | async-done | bytes 1048608 | tf_op jit(solution)/shard_map/all_to_all | solution.py:426
  335.7 0.1 copy.43
  336.0 3.9 %fusion.39 = (bf16[2048,1024]{1,0:T(8,128)(2,1)S(1)}, bf16[2048,1024]{1,0:T(8,128)(2,1)S(1)}) fusion(bf16[4096,1024]{1,0:T(8,128)(2,1)} %all-gather.6.cloned.1.call-done), kind=kLoop, calls=%fused_computation.49 | loop fusion | bytes 16777216 | tf_op jit(solution)/shard_map/slice | solution.py:440
  339.9 0.7 fusion.4
  340.6 0.7 fusion.12
  341.4 0.7 fusion
  342.2 1.5 fusion.21
  (48 shorter events, 0.7 us)
Async XLA Ops:
  6.5 124.6 %copy-start.1 = (f32[256,1024]{1,0:T(8,128)S(1)}, f32[256,1024]{1,0:T(8,128)}, u32[]{:S(2)}) copy-start(f32[256,1024]{1,0:T(8,128)} %param.26) | copy-start | bytes 3145732
  6.5 124.6 %all-gather.8.cloned.1.call-start = ((), (), s32[]{:S(2)}) async-start(), calls=%async_computation.4 | async-start | bytes 17301504 | tf_op jit(solution)/shard_map/all_gather | solution.py:392
  14.1 321.9 %all-gather.6.cloned.1.call-start = ((), (), s32[]{:S(2)}) async-start(), calls=%async_computation.3 | async-start | bytes 8912896 | tf_op jit(solution)/shard_map/all_gather | solution.py:394
  131.2 5.3 %copy-start.2 = (bf16[128,1024]{1,0:T(8,128)(2,1)S(1)}, bf16[128,1024]{1,0:T(8,128)(2,1)}, u32[]{:S(2)}) copy-start(bf16[128,1024]{1,0:T(8,128)(2,1)} %param.17) | copy-start | bytes 786436
  131.2 5.5 %copy-start.3 = (bf16[128,1024]{1,0:T(8,128)(2,1)S(1)}, bf16[128,1024]{1,0:T(8,128)(2,1)}, u32[]{:S(2)}) copy-start(bf16[128,1024]{1,0:T(8,128)(2,1)} %param.18) | copy-start | bytes 786436
  132.5 4.4 %copy-start.4 = (bf16[128,1024]{1,0:T(8,128)(2,1)S(1)}, bf16[128,1024]{1,0:T(8,128)(2,1)}, u32[]{:S(2)}) copy-start(bf16[128,1024]{1,0:T(8,128)(2,1)} %param.19) | copy-start | bytes 786436
  132.5 4.6 %copy-start.5 = (bf16[128,1024]{1,0:T(8,128)(2,1)S(1)}, bf16[128,1024]{1,0:T(8,128)(2,1)}, u32[]{:S(2)}) copy-start(bf16[128,1024]{1,0:T(8,128)(2,1)} %param.20) | copy-start | bytes 786436
  132.5 4.8 %copy-start.6 = (bf16[128,1024]{1,0:T(8,128)(2,1)S(1)}, bf16[128,1024]{1,0:T(8,128)(2,1)}, u32[]{:S(2)}) copy-start(bf16[128,1024]{1,0:T(8,128)(2,1)} %param.21) | copy-start | bytes 786436
  132.5 4.9 %copy-start.7 = (bf16[128,1024]{1,0:T(8,128)(2,1)S(1)}, bf16[128,1024]{1,0:T(8,128)(2,1)}, u32[]{:S(2)}) copy-start(bf16[128,1024]{1,0:T(8,128)(2,1)} %param.22) | copy-start | bytes 786436
  132.5 39.8 %all-to-all-start.1 = ((f32[16,256,64]{1,2,0:T(8,128)}), f32[16,256,64]{1,2,0:T(8,128)S(1)}, u32[]{:S(2)}, u32[]{:S(2)}) async-start(f32[16,256,64]{1,2,0:T(8,128)} %bitcast.16), calls=%async_computation.1 | async-start | bytes 2097152 | tf_op jit(solution)/shard_map/all_to_all | solution.py:415
  136.5 1.1 copy-start.8
  139.5 38.9 %copy-start.9 = (bf16[3,1024]{1,0:T(4,128)(2,1)S(1)}, bf16[3,1024]{1,0:T(4,128)(2,1)}, u32[]{:S(2)}) copy-start(bf16[3,1024]{1,0:T(4,128)(2,1)} %param.24) | copy-start | bytes 18436
  139.5 38.9 %copy-start.10 = (f32[1024]{0:T(1024)S(1)}, f32[1024]{0:T(1024)}, u32[]{:S(2)}) copy-start(f32[1024]{0:T(1024)} %param.25) | copy-start | bytes 12292
  139.5 38.9 %copy-start.11 = (f32[1024]{0:T(1024)S(1)}, f32[1024]{0:T(1024)}, u32[]{:S(2)}) copy-start(f32[1024]{0:T(1024)} %param.27) | copy-start | bytes 12292
  139.5 38.9 %copy-start.12 = (f32[1024]{0:T(1024)S(1)}, f32[1024]{0:T(1024)}, u32[]{:S(2)}) copy-start(f32[1024]{0:T(1024)} %param.28) | copy-start | bytes 12292
  172.4 62.3 %all-to-all-start = ((bf16[16,128,448]{1,2,0:T(8,128)(2,1)}), bf16[16,128,448]{1,2,0:T(8,128)(2,1)}, u32[]{:S(2)}, u32[]{:S(2)}) async-start(bf16[16,128,448]{1,2,0:T(8,128)(2,1)} %bitcast.13), calls=%async_computation | async-start | bytes 3670016 | tf_op jit(solution)/shard_map/all_to_all | solution.py:412
  238.6 1.6 copy-start
  292.2 43.6 %all-to-all-start.2 = ((bf16[16,256,128]{1,2,0:T(8,128)(2,1)}), bf16[16,256,128]{1,2,0:T(8,128)(2,1)S(1)}, u32[]{:S(2)}, u32[]{:S(2)}) async-start(bf16[16,256,128]{1,2,0:T(8,128)(2,1)} %copy.42), calls=%async_computation.2 | async-start | bytes 2097152 | tf_op jit(solution)/shard_map/all_to_all | solution.py:426
  335.8 5.6 %collective-permute-start = (bf16[256,2048]{0,1:T(8,128)(2,1)S(1)}, bf16[256,2048]{0,1:T(8,128)(2,1)S(1)}, u32[]{:S(2)}, u32[]{:S(2)}) collective-permute-start(bf16[256,2048]{0,1:T(8,128)(2,1)S(1)} %bitcast.64), channel_id=1, source_target_pairs={{0,1},{1,0},{2,3},{3,2},{4,5},{5,4},{6,7},{7,6},{8,9},{9,8},{10,11... | collective-permute-start | bytes 3145736 | tf_op jit(solution)/shard_map/ppermute | solution.py:433
Sparse Core Ops, SparseCore 0:
  14.2 116.8 all-gather.7
  133.9 153.7 all-gather.5

commit v3 on v2

--- a/solution.py
+++ b/solution.py
@@ -390,10 +390,6 @@
         (wide - center[:, None]) * lax.rsqrt(variance + norm_eps)[:, None] * gain
     ).astype(jnp.bfloat16)
     normed = lax.all_gather(normed, ("sp", "tp"), axis=0)
-    normed, readout_projector = lax.optimization_barrier((normed, readout_projector))
-    output_rows = lax.all_gather(readout_projector, "sp", axis=0, tiled=True)
-    output_rows = output_rows.reshape(2, halves, cols, cols)
-    normed = normed.reshape(count, halves, rows, cols)
 
     weights = jnp.stack(
         [
@@ -410,9 +406,16 @@
     weights = weights.reshape(kinds, depth, count, HEAD_SIZE).transpose(2, 1, 0, 3)
     weights = weights.reshape(count, depth, kinds * HEAD_SIZE)
     weights = lax.all_to_all(weights, "sp", 0, 0, tiled=True)
+    shift = decay_shift.reshape(rows, count, HEAD_SIZE).transpose(1, 0, 2)
+    shift = lax.all_to_all(shift, "sp", 0, 0, tiled=True)
+    normed, weights, shift, readout_projector = lax.optimization_barrier(
+        (normed, weights, shift, readout_projector)
+    )
+    output_rows = lax.all_gather(readout_projector, "sp", axis=0, tiled=True)
+    output_rows = output_rows.reshape(2, halves, cols, cols)
+    normed = normed.reshape(count, halves, rows, cols)
     weights = weights.reshape(halves, cols, kinds * HEAD_SIZE)
-    shift = decay_shift.reshape(rows, count, HEAD_SIZE).transpose(1, 0, 2)
-    shift = lax.all_to_all(shift, "sp", 0, 0, tiled=True).reshape(count * rows, HEAD_SIZE)
+    shift = shift.reshape(count * rows, HEAD_SIZE)
     vectors = jnp.concatenate(
         [
             jnp.stack([decay_base, rate_logit, head_gain]),

time: 351 us -> 323 us (0.920)
  waiting for transfers between devices: 227 us -> 146 us
  blocking collectives: 1.99 us -> 75.9 us
  starting transfers between devices: 31.6 us -> 13 us
    all_gather x1, waiting for transfers between devices: 117 us -> 40.8 us  [head_body(): normed = lax.all_gather(normed, ('sp', 'tp'), axis=0)]
    all_to_all x0 -> x1, blocking collectives: none -> 73.9 us  [head_body(): weights = lax.all_to_all(weights, 'sp', 0, 0, tiled=True)]
    all_to_all x2 -> x1, waiting for transfers between devices: 88.2 us -> 34 us  [head_body(): shift = lax.all_to_all(shift, 'sp', 0, 0, tiled=True)]
    all_gather x1, waiting for transfers between devices: 0.02 us -> 30.5 us  [head_body(): output_rows = lax.all_gather(readout_projector, 'sp', axis=0, tiled=True)]
    all_to_all x1, waiting for transfers between devices: 22.1 us -> 40.6 us  [head_body(): branches = lax.all_to_all(branches, 'sp', 0, 0, tiled=True)]
    all_to_all x1, starting transfers between devices: 21.5 us -> 4.52 us  [head_body(): branches = lax.all_to_all(branches, 'sp', 0, 0, tiled=True)]
    all_to_all x2 -> x0, local copies, waits for them, and re-layouts: 4.6 us -> none  [the longest x1 4 us: head_body(): weights = lax.all_to_all(weights, 'sp', 0, 0, tiled=True)]
    optimization_barrier x0 -> x2, local copies, waits for them, and re-layouts: none -> 4.4 us  [head_body(): lax.optimization_barrier((normed, weights, shift, readout_projector))]
  transfers between devices with their start and end apart: 6 -> 5, of which waited for: 4 -> 4; matrix products, arithmetic and copies ran while one was open for 4% -> 4% of each run, Pallas kernels for 14% -> 16%
where the time goes in v3:
time: 323 us
  waiting for transfers between devices  146 us (45%)
  blocking collectives  75.9 us (23%)
  Pallas kernels  50.6 us (16%)
  local copies, waits for them, and re-layouts  15.1 us (5%)
  between operations  13.8 us (4%)
  starting transfers between devices  13 us (4%)
  other arithmetic  4.81 us (1%)
  matrix products  3.78 us (1%)
    all_to_all x1, blocking collectives, head_body(): weights = lax.all_to_all(weights, 'sp', 0, 0, tiled=True)  73.9 us
    pallas_call x1, Pallas kernels, run_mixer(): pl.pallas_call(mixer_kernel, grid=(length // rows,), out_shape=jax.ShapeD...  50.6 us
    all_gather x1, waiting for transfers between devices, head_body(): normed = lax.all_gather(normed, ('sp', 'tp'), axis=0)  40.8 us
    all_to_all x1, waiting for transfers between devices, head_body(): branches = lax.all_to_all(branches, 'sp', 0, 0, tiled=True)  40.6 us
    all_to_all x1, waiting for transfers between devices, head_body(): shift = lax.all_to_all(shift, 'sp', 0, 0, tiled=True)  34 us
    all_gather x1, waiting for transfers between devices, head_body(): output_rows = lax.all_gather(readout_projector, 'sp', axis=0, tiled=True)  30.5 us
    all_to_all x1, starting transfers between devices, head_body(): shift = lax.all_to_all(shift, 'sp', 0, 0, tiled=True)  8.34 us
  transfers between devices with their start and end apart: 5, of which 4 were waited for; matrix products, arithmetic and copies ran while one was open for 4% of the time, Pallas kernels for 16%

profile of v3, /device:TPU:0, one launch (start us, length us, event | category | flops | bytes accessed | tf_op | source)
XLA Modules:
  0.0 322.8 jit_solution(17299304305755106553)
XLA Ops:
  6.5 1.3 convert_reduce_fusion
  7.8 1.3 fusion.25
  9.2 2.0 all-gather.2
  11.2 0.7 dynamic_slice.19
  11.9 2.1 fusion.28
  14.1 1.3 copy.39
  15.4 8.3 %all-to-all-start.1 = ((f32[16,256,64]{1,2,0:T(8,128)}), f32[16,256,64]{1,2,0:T(8,128)S(1)}, u32[]{:S(2)}, u32[]{:S(2)}) async-start(f32[16,256,64]{1,2,0:T(8,128)} %bitcast.14), calls=%async_computation.1 | async-start | bytes 2097152 | tf_op jit(solution)/shard_map/all_to_all | solution.py:410
  23.9 0.2 copy.31
  24.0 0.2 copy.32
  24.2 0.2 copy.33
  24.4 0.2 copy.34
  24.6 0.2 copy.35
  24.8 0.2 copy.36
  25.0 0.2 copy.37
  25.4 0.1 copy.38
  25.6 34.0 %all-to-all-done.1 = f32[16,256,64]{1,2,0:T(8,128)S(1)} async-done(((f32[16,256,64]{1,2,0:T(8,128)}), f32[16,256,64]{1,2,0:T(8,128)S(1)}, u32[]{:S(2)}, u32[]{:S(2)}) %all-to-all-start.1) | async-done | bytes 1048608 | tf_op jit(solution)/shard_map/all_to_all | solution.py:410
  59.6 73.9 %all_to_all.15 = bf16[16,128,448]{1,2,0:T(8,128)(2,1)} all-to-all(bf16[16,128,448]{1,2,0:T(8,128)(2,1)S(1)} %bitcast.63), channel_id=1, replica_groups=mesh['sp'=16,'tp'=2] {'sp'}, dimensions={0} | all-to-all | bytes 3670016 | tf_op jit(solution)/shard_map/all_to_all | solution.py:408
  133.5 40.8 %all-gather.8.cloned.1.call-done = bf16[8192,1024]{1,0:T(8,128)(2,1)} async-done(((bf16[256,1024]{1,0:T(8,128)(2,1)}), bf16[8192,1024]{1,0:T(8,128)(2,1)}) %all-gather.8.cloned.1.call-update) | async-done | bytes 16777232 | tf_op jit(solution)/shard_map/all_gather | solution.py:392
  174.4 3.8 %copy.40 = bf16[16,128,448]{2,1,0:T(8,128)(2,1)} copy(bf16[16,128,448]{1,2,0:T(8,128)(2,1)} %all_to_all.15) | data formatting | bytes 3670016 | tf_op jit(solution)/shard_map/optimization_barrier | solution.py:411
  178.2 0.6 copy.41
  178.9 1.6 copy-done
  180.4 50.6 %shard_map.145 = bf16[4096,128]{1,0:T(8,128)(2,1)S(1)} custom-call(bf16[16,2,256,1024]{3,2,1,0:T(8,128)(2,1)} %bitcast.81, bf16[2,1024,448]{2,1,0:T(8,128)(2,1)S(1)} %bitcast.57, f32[4096,64]{1,0:T(8,128)S(1)} %bitcast.56, f32[8,64]{1,0:T(8,128)S(1)} %constant_dynamic-slice_fusion.vec_ref), custom_call_target="tpu_custom_call" | custom-call | flops 60000002048 | bytes 16777216 | tf_op jit(solution)/shard_map/pallas_call | solution.py:333
  231.1 1.3 copy.42
  232.4 4.5 %all-to-all-start.2 = ((bf16[16,256,128]{1,2,0:T(8,128)(2,1)}), bf16[16,256,128]{1,2,0:T(8,128)(2,1)S(1)}, u32[]{:S(2)}, u32[]{:S(2)}) async-start(bf16[16,256,128]{1,2,0:T(8,128)(2,1)} %copy.42), calls=%async_computation.2 | async-start | bytes 2097152 | tf_op jit(solution)/shard_map/all_to_all | solution.py:429
  236.9 40.6 %all-to-all-done.2 = bf16[16,256,128]{1,2,0:T(8,128)(2,1)S(1)} async-done(((bf16[16,256,128]{1,2,0:T(8,128)(2,1)}), bf16[16,256,128]{1,2,0:T(8,128)(2,1)S(1)}, u32[]{:S(2)}, u32[]{:S(2)}) %all-to-all-start.2) | async-done | bytes 1048608 | tf_op jit(solution)/shard_map/all_to_all | solution.py:429
  277.5 0.1 copy.43
  277.7 30.5 %all-gather.6.cloned.1.call-done = bf16[4096,1024]{1,0:T(8,128)(2,1)} async-done(((bf16[256,1024]{1,0:T(8,128)(2,1)}), bf16[4096,1024]{1,0:T(8,128)(2,1)}) %all-gather.6.cloned.1.call-update) | async-done | bytes 8388624 | tf_op jit(solution)/shard_map/all_gather | solution.py:414
  308.2 3.9 %fusion.39 = (bf16[2048,1024]{1,0:T(8,128)(2,1)S(1)}, bf16[2048,1024]{1,0:T(8,128)(2,1)S(1)}) fusion(bf16[4096,1024]{1,0:T(8,128)(2,1)} %all-gather.6.cloned.1.call-done), kind=kLoop, calls=%fused_computation.49 | loop fusion | bytes 16777216 | tf_op jit(solution)/shard_map/slice | solution.py:443
  312.1 0.7 fusion.4
  312.9 0.7 fusion.12
  313.7 0.7 fusion
  314.4 1.6 fusion.21
  (47 shorter events, 0.6 us)
Async XLA Ops:
  6.5 7.5 %copy-start.1 = (f32[256,1024]{1,0:T(8,128)S(1)}, f32[256,1024]{1,0:T(8,128)}, u32[]{:S(2)}) copy-start(f32[256,1024]{1,0:T(8,128)} %param.26) | copy-start | bytes 3145732
  6.5 167.7 %all-gather.8.cloned.1.call-start = ((), (), s32[]{:S(2)}) async-start(), calls=%async_computation.4 | async-start | bytes 17301504 | tf_op jit(solution)/shard_map/all_gather | solution.py:392
  14.1 9.8 %copy-start.2 = (bf16[128,1024]{1,0:T(8,128)(2,1)S(1)}, bf16[128,1024]{1,0:T(8,128)(2,1)}, u32[]{:S(2)}) copy-start(bf16[128,1024]{1,0:T(8,128)(2,1)} %param.17) | copy-start | bytes 786436
  14.1 9.9 %copy-start.3 = (bf16[128,1024]{1,0:T(8,128)(2,1)S(1)}, bf16[128,1024]{1,0:T(8,128)(2,1)}, u32[]{:S(2)}) copy-start(bf16[128,1024]{1,0:T(8,128)(2,1)} %param.18) | copy-start | bytes 786436
  15.4 8.8 %copy-start.4 = (bf16[128,1024]{1,0:T(8,128)(2,1)S(1)}, bf16[128,1024]{1,0:T(8,128)(2,1)}, u32[]{:S(2)}) copy-start(bf16[128,1024]{1,0:T(8,128)(2,1)} %param.19) | copy-start | bytes 786436
  15.4 9.0 %copy-start.5 = (bf16[128,1024]{1,0:T(8,128)(2,1)S(1)}, bf16[128,1024]{1,0:T(8,128)(2,1)}, u32[]{:S(2)}) copy-start(bf16[128,1024]{1,0:T(8,128)(2,1)} %param.20) | copy-start | bytes 786436
  15.4 9.2 %copy-start.6 = (bf16[128,1024]{1,0:T(8,128)(2,1)S(1)}, bf16[128,1024]{1,0:T(8,128)(2,1)}, u32[]{:S(2)}) copy-start(bf16[128,1024]{1,0:T(8,128)(2,1)} %param.21) | copy-start | bytes 786436
  15.4 9.3 %copy-start.7 = (bf16[128,1024]{1,0:T(8,128)(2,1)S(1)}, bf16[128,1024]{1,0:T(8,128)(2,1)}, u32[]{:S(2)}) copy-start(bf16[128,1024]{1,0:T(8,128)(2,1)} %param.22) | copy-start | bytes 786436
  15.4 44.1 %all-to-all-start.1 = ((f32[16,256,64]{1,2,0:T(8,128)}), f32[16,256,64]{1,2,0:T(8,128)S(1)}, u32[]{:S(2)}, u32[]{:S(2)}) async-start(f32[16,256,64]{1,2,0:T(8,128)} %bitcast.14), calls=%async_computation.1 | async-start | bytes 2097152 | tf_op jit(solution)/shard_map/all_to_all | solution.py:410
  23.8 1.2 copy-start.8
  23.8 284.4 %all-gather.6.cloned.1.call-start = ((), (), s32[]{:S(2)}) async-start(), calls=%async_computation.3 | async-start | bytes 8912896 | tf_op jit(solution)/shard_map/all_gather | solution.py:414
  59.6 114.7 %copy-start.9 = (bf16[3,1024]{1,0:T(4,128)(2,1)S(1)}, bf16[3,1024]{1,0:T(4,128)(2,1)}, u32[]{:S(2)}) copy-start(bf16[3,1024]{1,0:T(4,128)(2,1)} %param.24) | copy-start | bytes 18436
  59.6 114.7 %copy-start.10 = (f32[1024]{0:T(1024)S(1)}, f32[1024]{0:T(1024)}, u32[]{:S(2)}) copy-start(f32[1024]{0:T(1024)} %param.25) | copy-start | bytes 12292
  59.6 114.7 %copy-start.11 = (f32[1024]{0:T(1024)S(1)}, f32[1024]{0:T(1024)}, u32[]{:S(2)}) copy-start(f32[1024]{0:T(1024)} %param.27) | copy-start | bytes 12292
  59.6 114.7 %copy-start.12 = (f32[1024]{0:T(1024)S(1)}, f32[1024]{0:T(1024)}, u32[]{:S(2)}) copy-start(f32[1024]{0:T(1024)} %param.28) | copy-start | bytes 12292
  178.8 1.6 copy-start
  232.4 45.1 %all-to-all-start.2 = ((bf16[16,256,128]{1,2,0:T(8,128)(2,1)}), bf16[16,256,128]{1,2,0:T(8,128)(2,1)S(1)}, u32[]{:S(2)}, u32[]{:S(2)}) async-start(bf16[16,256,128]{1,2,0:T(8,128)(2,1)} %copy.42), calls=%async_computation.2 | async-start | bytes 2097152 | tf_op jit(solution)/shard_map/all_to_all | solution.py:429
  277.6 36.0 %collective-permute-start = (bf16[256,2048]{0,1:T(8,128)(2,1)S(1)}, bf16[256,2048]{0,1:T(8,128)(2,1)S(1)}, u32[]{:S(2)}, u32[]{:S(2)}) collective-permute-start(bf16[256,2048]{0,1:T(8,128)(2,1)S(1)} %bitcast.65), channel_id=1, source_target_pairs={{0,1},{1,0},{2,3},{3,2},{4,5},{5,4},{6,7},{7,6},{8,9},{9,8},{10,11... | collective-permute-start | bytes 3145736 | tf_op jit(solution)/shard_map/ppermute | solution.py:436
Sparse Core Ops, SparseCore 0:
  14.2 159.9 all-gather.7
  177.0 131.1 all-gather.5
